TPU v7x, 32 devices: a whole 2x2x4 slice. The times are simulated.
32 devices in a mesh: grp: 2 (over y), sp: 4 (over z), tp: 4 (over x, core).
Axes of the slice: x: 2, y: 2, z: 4, core: 2. Of those that a mesh axis runs over, the one named last changes fastest.
Arguments:
- resid_in: bfloat16 [2048, 2048], P(('grp', 'sp', 'tp')), parts along dimension 0, may hold values from -6 to 6
- query_narrow: bfloat16 [2048, 8, 128], P(('grp', 'sp'), 'tp'), parts along dimension 0, may hold values from -512 to 512
- key_narrow: bfloat16 [2048, 4, 128], P(('grp', 'sp'), 'tp'), parts along dimension 0, may hold values from -512 to 512
- value_narrow: bfloat16 [2048, 4, 128], P(('grp', 'sp'), 'tp'), parts along dimension 0, may hold values from -6 to 6
- query_wide: bfloat16 [2048, 8, 256], P(('grp', 'sp'), 'tp'), parts along dimension 0, may hold values from -512 to 512
- key_wide: bfloat16 [2048, 4, 256], P(('grp', 'sp'), 'tp'), parts along dimension 0, may hold values from -512 to 512
- value_wide: bfloat16 [2048, 4, 128], P(('grp', 'sp'), 'tp'), parts along dimension 0, may hold values from -6 to 6
- lambda_narrow: float32 [8], P('tp'), may hold values from 0.3 to 0.8
- lambda_wide: float32 [8], P('tp'), may hold values from 0.3 to 0.8
- head_gain: float32 [128], replicated, may hold values from 0.1 to 1.9
- out_narrow: bfloat16 [1024, 2048], P('tp'), may hold values from -0.125 to 0.125
- out_wide: bfloat16 [1024, 2048], P('tp'), may hold values from -0.125 to 0.125
- norm_gain: bfloat16 [2048], replicated, may hold values from 0.099609375 to 1.8984375
- up_weight: bfloat16 [2048, 8192], P('sp', 'tp'), may hold values from -0.125 to 0.125
- down_weight: bfloat16 [8192, 2048], P('tp', 'sp'), may hold values from -0.0625 to 0.0625
Outputs:
- mixed_out: bfloat16 [2048, 2048], P(('grp', 'sp', 'tp')), parts along dimension 0
There are 2 independent parts, one for each index of `grp`. A program takes and returns all parts, laid end to end along the dimension named above; an argument that names none is the same for every part. Nothing has to cross between parts.
All inputs are finite; a program needn't handle non-finite values.
Results may differ from a plain program's by a relative error of at most 0.018.
Values may be sent and summed in bfloat16 or wider, within the bound.
A program may use at most 128 MiB of HBM per device.

v0:
```python
import math
import jax
import jax.numpy as jnp
from jax import lax
from jax.sharding import PartitionSpec as P

NORM_EPS = 1e-06
OUT_SCALE = 0.8


def empty_state(query, key_head_stack, value_width):
    row_count, head_count = (query.shape[0], query.shape[1])
    group_size = head_count // key_head_stack
    row_top = jnp.full((key_head_stack, group_size, 2, row_count), -jnp.inf, jnp.float32)
    row_total = jnp.zeros((key_head_stack, group_size, 2, row_count), jnp.float32)
    weighted_values = jnp.zeros(
        (key_head_stack, group_size, 2, row_count, value_width), jnp.float32
    )
    return (row_top, row_total, weighted_values)


def absorb(states, query, key_rows, values):
    row_count, head_count = (query.shape[0], query.shape[1])
    key_head_stack = key_rows.shape[1]
    half_width = key_rows.shape[2] // 2
    group_size = head_count // key_head_stack
    value_width = values.shape[2]
    amount = key_rows.shape[0]
    block_rows = math.gcd(amount, 512)
    rotation_count = amount // block_rows
    grouped = query.reshape(row_count, key_head_stack, group_size, 2, half_width)
    key_block_list = key_rows.reshape(rotation_count, block_rows, key_head_stack, 2, half_width)
    value_blocks = values.reshape(rotation_count, block_rows, key_head_stack, value_width)

    def visit(running, kv_pair):
        row_top, row_total, weighted_values = running
        key_blk, value_blk = kv_pair
        scores = jnp.einsum(
            "tkgcd,skcd->kgcts", grouped, key_blk, preferred_element_type=jnp.float32
        ) * half_width ** (-0.5)
        new_top = jnp.maximum(row_top, jnp.max(scores, axis=-1))
        rescale = jnp.exp(row_top - new_top)
        powers = jnp.exp(scores - new_top[..., None])
        row_total = row_total * rescale + jnp.sum(powers, axis=-1)
        weighted_values = weighted_values * rescale[..., None] + jnp.einsum(
            "iodph,hie->iodpe",
            powers.astype(jnp.bfloat16),
            value_blk,
            preferred_element_type=jnp.float32,
        )
        return ((new_top, row_total, weighted_values), None)

    outcome, _ = lax.scan(visit, states, (key_block_list, value_blocks))
    return outcome


def finish(states, lambdas, gain_vec):
    row_top, row_total, weighted_values = states
    key_head_stack, group_size, row_count = (row_top.shape[0], row_top.shape[1], row_top.shape[3])
    value_width = weighted_values.shape[4]
    first_map = weighted_values[:, :, 0] / row_total[:, :, 0, :, None]
    second_map = weighted_values[:, :, 1] / row_total[:, :, 1, :, None]
    mixed = first_map - lambdas.reshape(key_head_stack, group_size)[:, :, None, None] * second_map
    normed = (
        mixed
        * lax.rsqrt(jnp.mean(mixed * mixed, axis=-1, keepdims=True) + NORM_EPS)
        * gain_vec
        * OUT_SCALE
    )
    normed = normed.astype(jnp.bfloat16).transpose(2, 0, 1, 3)
    return normed.reshape(row_count, key_head_stack * group_size * value_width)


def attend(
    query_narrow,
    key_narrow,
    value_narrow,
    query_wide,
    key_wide,
    value_wide,
    lambda_narrow,
    lambda_wide,
    head_gain,
):
    initial = (
        empty_state(query_narrow, key_narrow.shape[1], value_narrow.shape[2]),
        empty_state(query_wide, key_wide.shape[1], value_wide.shape[2]),
    )
    narrow_keys = lax.all_gather(key_narrow, "sp", axis=0, tiled=True)
    narrow_values = lax.all_gather(value_narrow, "sp", axis=0, tiled=True)
    wide_keys = lax.all_gather(key_wide, "sp", axis=0, tiled=True)
    wide_values = lax.all_gather(value_wide, "sp", axis=0, tiled=True)
    narrow_state = absorb(initial[0], query_narrow, narrow_keys, narrow_values)
    wide_state = absorb(initial[1], query_wide, wide_keys, wide_values)
    return (
        finish(narrow_state, lambda_narrow, head_gain),
        finish(wide_state, lambda_wide, head_gain),
    )


def shards(
    resid_in,
    query_narrow,
    key_narrow,
    value_narrow,
    query_wide,
    key_wide,
    value_wide,
    lambda_narrow,
    lambda_wide,
    head_gain,
    out_narrow,
    out_wide,
    norm_gain,
    up_weight,
    down_weight,
):
    att_narrow, att_wide = attend(
        query_narrow,
        key_narrow,
        value_narrow,
        query_wide,
        key_wide,
        value_wide,
        lambda_narrow,
        lambda_wide,
        head_gain,
    )
    projected = lax.psum_scatter(
        (
            jnp.dot(att_narrow, out_narrow, preferred_element_type=jnp.float32)
            + jnp.dot(att_wide, out_wide, preferred_element_type=jnp.float32)
        ).astype(jnp.bfloat16),
        "tp",
        scatter_dimension=0,
        tiled=True,
    ).astype(jnp.float32)
    middle = (resid_in.astype(jnp.float32) + projected).astype(jnp.bfloat16)
    middle_f32 = middle.astype(jnp.float32)
    normed = middle_f32 * lax.rsqrt(
        jnp.mean(middle_f32 * middle_f32, axis=-1, keepdims=True) + NORM_EPS
    )
    normed = (normed * norm_gain.astype(jnp.float32)).astype(jnp.bfloat16)
    whole_rows = lax.all_gather(normed, "tp", axis=0, tiled=True)
    up_collected = lax.all_gather(up_weight, "sp", axis=0, tiled=True)
    lifted = jnp.dot(whole_rows, up_collected, preferred_element_type=jnp.float32)
    activated = jnp.square(jax.nn.relu(lifted)).astype(jnp.bfloat16)
    partials = jnp.dot(
        activated,
        lax.all_gather(down_weight, "sp", axis=1, tiled=True),
        preferred_element_type=jnp.float32,
    )
    mixer_out = lax.psum_scatter(
        partials.astype(jnp.bfloat16), "tp", scatter_dimension=0, tiled=True
    ).astype(jnp.float32)
    return (middle_f32 + mixer_out).astype(jnp.bfloat16)


def solution(mesh):
    placed = (
        P(("grp", "sp", "tp"), None),
        P(("grp", "sp"), "tp", None),
        P(("grp", "sp"), "tp", None),
        P(("grp", "sp"), "tp", None),
        P(("grp", "sp"), "tp", None),
        P(("grp", "sp"), "tp", None),
        P(("grp", "sp"), "tp", None),
        P("tp"),
        P("tp"),
        P(),
        P("tp", None),
        P("tp", None),
        P(),
        P("sp", "tp"),
        P("tp", "sp"),
    )
    return jax.shard_map(
        shards, mesh=mesh, in_specs=placed, out_specs=P(("grp", "sp", "tp"), None), check_vma=False
    )
```

profile of v0, /device:TPU:0, one launch (start us, length us, event | category | flops | bytes accessed | tf_op | source)
XLA Modules:
  0.0 480.9 jit_solution(12649065433829812458)
XLA Ops:
  6.6 17.7 %all_gather.23 = bf16[1024,1,256]{2,0,1:T(8,128)(2,1)S(1)} all-gather(bf16[256,1,256]{2,0,1:T(8,128)(2,1)} %param.24), channel_id=1, replica_groups=mesh['grp'=2,'sp'=4,'tp'=4] {'sp'}, dimensions={0}, use_global_device_ids=true | all-gather | bytes 655360 | tf_op jit(solution)/shard_map/all_gather | solution.py:91
  24.3 0.1 reshape.256
  24.4 1.1 copy.33
  25.5 0.2 copy.35
  25.7 15.3 %all_gather.24 = bf16[1024,1,128]{2,0,1:T(8,128)(2,1)} all-gather(bf16[256,1,128]{2,0,1:T(8,128)(2,1)S(1)} %copy-done.9), channel_id=1, replica_groups=mesh['grp'=2,'sp'=4,'tp'=4] {'sp'}, dimensions={0}, use_global_device_ids=true | all-gather | bytes 327680 | tf_op jit(solution)/shard_map/all_gather | solution.py:92
  41.1 8.2 %while.31 = (s32[]{:T(128)}, f32[1,2,2,256]{3,1,2,0:T(2,128)S(1)}, f32[1,2,2,256]{3,1,2,0:T(2,128)S(1)}, f32[1,2,2,256,128]{4,3,2,1,0:T(8,128)}, bf16[2,512,1,2,...) while((s32[]{:T(128)}, f32[1,2,2,256]{3,1,2,0:T(2,128)S(1)}, ...), condition=%wide.region_8.9_spmd.clone, body=%wide.region_5.0_spmd.clone.sunk | while | flops 271980544 | bytes 13832389 | solution.py:53
  41.1 0.2 constant_dynamic-slice_fusion.2
  41.3 0.6 copy-done.1
  41.9 0.4 bitcast_reduce_fusion.5
  42.4 0.4 fusion.71
  42.8 0.5 copy-done.7
  43.3 1.3 fusion.72
  44.7 0.2 constant_dynamic-slice_fusion.2
  44.9 0.6 copy-done.1
  45.5 0.4 bitcast_reduce_fusion.5
  46.0 0.4 fusion.71
  46.4 0.5 copy-done.7
  46.9 2.3 fusion.72
  49.3 0.0 copy-start.8
  49.3 0.6 slice_bitcast_fusion.5
  49.9 14.2 %all_gather.21 = bf16[1024,1,128]{2,0,1:T(8,128)(2,1)S(1)} all-gather(bf16[256,1,128]{2,0,1:T(8,128)(2,1)S(1)} %copy-done.10), channel_id=1, replica_groups=mesh['grp'=2,'sp'=4,'tp'=4] {'sp'}, dimensions={0}, use_global_device_ids=true | all-gather | bytes 327680 | tf_op jit(solution)/shard_map/all_gather | solution.py:89
  64.1 0.2 reshape.272
  64.3 0.4 copy.29
  64.7 15.6 %all_gather.22 = bf16[1024,1,128]{2,0,1:T(8,128)(2,1)} all-gather(bf16[256,1,128]{2,0,1:T(8,128)(2,1)} %param.22), channel_id=1, replica_groups=mesh['grp'=2,'sp'=4,'tp'=4] {'sp'}, dimensions={0}, use_global_device_ids=true | all-gather | bytes 327680 | tf_op jit(solution)/shard_map/all_gather | solution.py:90
  80.4 0.1 copy.28
  80.5 6.6 %while.30 = (s32[]{:T(128)}, f32[1,2,2,256]{3,1,2,0:T(2,128)S(1)}, f32[1,2,2,256]{3,1,2,0:T(2,128)S(1)}, f32[1,2,2,256,128]{4,3,2,1,0:T(8,128)}, bf16[2,512,1,2,...) while((s32[]{:T(128)}, f32[1,2,2,256]{3,1,2,0:T(2,128)S(1)}, ...), condition=%wide.region_3.4_spmd.clone, body=%wide.region_0.3_spmd.clone.sunk | while | flops 204871680 | bytes 8851597 | solution.py:53
  80.5 0.5 bitcast_reduce_fusion.4
  81.1 0.4 fusion.66
  81.5 0.5 copy-done.6
  82.0 1.3 fusion.67
  83.3 0.5 bitcast_reduce_fusion.4
  83.9 0.4 fusion.66
  84.3 0.5 copy-done.6
  84.8 2.3 fusion.67
  87.2 0.0 copy-start.11
  87.2 0.0 copy-start.13
  87.2 0.0 copy-start.14
  87.2 0.0 copy-start.15
  87.2 1.2 copy.36
  88.5 1.2 copy.31
  89.7 0.2 multiply_reduce_fusion
  89.9 0.0 copy-start.5
  90.0 0.1 multiply_convert_fusion
  90.1 0.5 fusion.45
  90.6 0.6 copy-done.5
  91.2 1.4 fusion.29
  92.6 0.0 reduce-scatter.3.cloned.1.call-update
  92.6 0.0 all-gather.4.cloned.1.call-start
  92.7 25.0 %reduce-scatter.3.cloned.1.call-done = bf16[64,2048]{1,0:T(8,128)(2,1)} async-done(((bf16[256,2048]{1,0:T(8,128)(2,1)}), bf16[64,2048]{1,0:T(8,128)(2,1)}) %reduce-scatter.3.cloned.1.call-update) | async-done | bytes 262160 | tf_op jit(solution)/shard_map/reduce_scatter | solution.py:129
  117.7 1.1 fusion.30
  118.8 1.8 fusion.32
  120.6 0.0 all-gather.4.cloned.1.call-update
  120.6 0.0 all-gather.6.cloned.1.call-start
  120.7 0.7 all-gather.6.cloned.1.call-update
  121.3 0.0 all-gather.8.cloned.1.call-start
  121.4 0.5 all-gather.8.cloned.1.call-update
  121.9 0.0 reduce-scatter.5.cloned.1.call-start
  122.0 15.5 %all-gather.4.cloned.1.call-done = bf16[256,2048]{1,0:T(8,128)(2,1)} async-done(((bf16[64,2048]{1,0:T(8,128)(2,1)}), bf16[256,2048]{1,0:T(8,128)(2,1)}) %all-gather.4.cloned.1.call-update) | async-done | bytes 1048592 | tf_op jit(solution)/shard_map/all_gather | solution.py:144
  137.4 151.2 %all-gather.6.cloned.1.call-done = bf16[2048,2048]{1,0:T(8,128)(2,1)} async-done(((bf16[512,2048]{1,0:T(8,128)(2,1)}), bf16[2048,2048]{1,0:T(8,128)(2,1)}) %all-gather.6.cloned.1.call-update) | async-done | bytes 8388624 | tf_op jit(solution)/shard_map/all_gather | solution.py:145
  288.7 149.3 %all-gather.8.cloned.1.call-done = bf16[2048,2048]{1,0:T(8,128)(2,1)} async-done(((bf16[2048,512]{1,0:T(8,128)(2,1)}), bf16[2048,2048]{1,0:T(8,128)(2,1)}) %all-gather.8.cloned.1.call-update) | async-done | bytes 8388624 | tf_op jit(solution)/shard_map/all_gather | solution.py:150
  437.9 11.5 %convolution_convert_fusion = bf16[256,2048]{1,0:T(8,128)(2,1)} fusion(bf16[2048,2048]{1,0:T(8,128)(2,1)} %all-gather.8.cloned.1.call-done, bf16[256,2048]{1,0:T(8,128)(2,1)} %all-gather.4.cloned.1.call-done, bf16[2048,2048]{1,0:T(8,128)(2,1)} %all-gather.6.cloned.1.call-done), kind=kOutput, calls=%fused_computation.52 | convolution fusion | flops 4297064448 | bytes 18874368 | tf_op jit(solution)/shard_map/dot_general | solution.py:148
  449.5 0.0 reduce-scatter.5.cloned.1.call-update
  449.5 23.1 %reduce-scatter.5.cloned.1.call-done = bf16[64,2048]{1,0:T(8,128)(2,1)} async-done(((bf16[256,2048]{1,0:T(8,128)(2,1)}), bf16[64,2048]{1,0:T(8,128)(2,1)}) %reduce-scatter.5.cloned.1.call-update) | async-done | bytes 262160 | tf_op jit(solution)/shard_map/reduce_scatter | solution.py:153
  472.6 1.7 fusion.33
  (56 shorter events, 0.2 us)
Async XLA Ops:
  6.5 83.6 %copy-start = (bf16[256,2048]{1,0:T(8,128)(2,1)S(1)}, bf16[256,2048]{1,0:T(8,128)(2,1)}, u32[]{:S(2)}) copy-start(bf16[256,2048]{1,0:T(8,128)(2,1)} %param.29) | copy-start | bytes 3145732
  6.5 19.2 %copy-start.9 = (bf16[256,1,128]{2,0,1:T(8,128)(2,1)S(1)}, bf16[256,1,128]{2,0,1:T(8,128)(2,1)}, u32[]{:S(2)}) copy-start(bf16[256,1,128]{2,0,1:T(8,128)(2,1)} %param.25) | copy-start | bytes 196612
  6.5 111.1 %reduce-scatter.3.cloned.1.call-start = ((), (), s32[]{:S(2)}) async-start(), calls=%async_computation.2 | async-start | bytes 1310720 | tf_op jit(solution)/shard_map/reduce_scatter | solution.py:129
  41.1 8.8 %copy-start.10 = (bf16[256,1,128]{2,0,1:T(8,128)(2,1)S(1)}, bf16[256,1,128]{2,0,1:T(8,128)(2,1)}, u32[]{:S(2)}) copy-start(bf16[256,1,128]{2,0,1:T(8,128)(2,1)} %param.21) | copy-start | bytes 196612
  41.1 0.8 copy-start.1
  42.4 1.0 copy-start.7
  42.8 1.8 copy-start.2
  44.7 0.8 copy-start.1
  45.9 1.0 copy-start.7
  46.4 2.9 copy-start.2
  49.3 31.1 %copy-start.8 = (bf16[256,2,128]{2,1,0:T(2,128)(2,1)S(1)}, bf16[256,2,128]{2,1,0:T(2,128)(2,1)}, u32[]{:S(2)}) copy-start(bf16[256,2,128]{2,1,0:T(2,128)(2,1)} %param.20) | copy-start | bytes 393220
  81.0 1.0 copy-start.6
  83.8 1.0 copy-start.6
  87.2 2.6 copy-start.11
  87.2 2.6 copy-start.13
  87.2 2.6 copy-start.14
  87.2 2.8 copy-start.15
  89.9 1.2 copy-start.5
  91.2 1.5 copy-start.12
  91.2 26.5 %copy-start.3 = (bf16[64,2048]{1,0:T(8,128)(2,1)S(1)}, bf16[64,2048]{1,0:T(8,128)(2,1)}, u32[]{:S(2)}) copy-start(bf16[64,2048]{1,0:T(8,128)(2,1)} %param.19) | copy-start | bytes 786436
  92.6 44.8 %all-gather.4.cloned.1.call-start = ((), (), s32[]{:S(2)}) async-start(), calls=%async_computation.3 | async-start | bytes 1310720 | tf_op jit(solution)/shard_map/all_gather | solution.py:144
  120.6 168.1 %all-gather.6.cloned.1.call-start = ((), (), s32[]{:S(2)}) async-start(), calls=%async_computation.4 | async-start | bytes 10485760 | tf_op jit(solution)/shard_map/all_gather | solution.py:145
  121.3 316.6 %all-gather.8.cloned.1.call-start = ((), (), s32[]{:S(2)}) async-start(), calls=%async_computation.5 | async-start | bytes 10485760 | tf_op jit(solution)/shard_map/all_gather | solution.py:150
  121.9 350.7 %copy-start.4 = (bf16[64,2048]{1,0:T(8,128)(2,1)S(1)}, bf16[64,2048]{1,0:T(8,128)(2,1)}, u32[]{:S(2)}) copy-start(bf16[64,2048]{1,0:T(8,128)(2,1)} %reduce-scatter.3.cloned.1.call-done) | copy-start | bytes 786436
  121.9 350.7 %reduce-scatter.5.cloned.1.call-start = ((), (), s32[]{:S(2)}) async-start(), calls=%async_computation.6 | async-start | bytes 1310720 | tf_op jit(solution)/shard_map/reduce_scatter | solution.py:153
Sparse Core Ops, SparseCore 0:
  92.7 24.8 reduce-scatter.2
  120.7 16.6 all-gather.3
  139.0 149.6 all-gather.5
  290.1 147.7 all-gather.7
  449.6 22.9 reduce-scatter.4
where the time goes:
time: 481 us
  waiting for transfers between devices  365 us (76%)
  blocking collectives  62.9 us (13%)
  matrix products  22.6 us (5%)
  between operations  13.4 us (3%)
  local copies, waits for them, and re-layouts  9.51 us (2%)
  other arithmetic  6.74 us (1%)
    all_gather x1, waiting for transfers between devices, shards(): up_collected = lax.all_gather(up_weight, 'sp', axis=0, tiled=True)  151 us
    all_gather x1, waiting for transfers between devices, shards(): lax.all_gather(down_weight, 'sp', axis=1, tiled=True)  149 us
    reduce_scatter x1, waiting for transfers between devices, shards(): lax.psum_scatter((jnp.dot(att_narrow, out_narrow, preferred_element_type=...  25 us
    reduce_scatter x1, waiting for transfers between devices, shards(): lax.psum_scatter(partials.astype(jnp.bfloat16), 'tp', scatter_dimension=0...  23.1 us
    all_gather x1, blocking collectives, attend(): wide_keys = lax.all_gather(key_wide, 'sp', axis=0, tiled=True)  17.7 us
    all_gather x1, blocking collectives, attend(): narrow_values = lax.all_gather(value_narrow, 'sp', axis=0, tiled=True)  15.6 us
    all_gather x1, waiting for transfers between devices, shards(): whole_rows = lax.all_gather(normed, 'tp', axis=0, tiled=True)  15.5 us
    all_gather x1, blocking collectives, attend(): wide_values = lax.all_gather(value_wide, 'sp', axis=0, tiled=True)  15.3 us
  transfers between devices with their start and end apart: 5, of which 5 were waited for; matrix products, arithmetic and copies ran while one was open for 0% of the time, Pallas kernels for 0%

commit v1 on v0

--- a/solution.py
+++ b/solution.py
@@ -147,7 +147,7 @@
     activated = jnp.square(jax.nn.relu(lifted)).astype(jnp.bfloat16)
     partials = jnp.dot(
         activated,
-        lax.all_gather(down_weight, "sp", axis=1, tiled=True),
+        jnp.concatenate(lax.all_gather(down_weight, "sp"), axis=1),
         preferred_element_type=jnp.float32,
     )
     mixer_out = lax.psum_scatter(

time: 481 us -> 456 us (0.948)
  waiting for transfers between devices: 365 us -> 327 us
  local copies, waits for them, and re-layouts: 9.51 us -> 24.7 us
    all_gather x1, waiting for transfers between devices: 149 us -> 123 us  [shards(): lax.all_gather(down_weight, 'sp')]
    reshape x0 -> x1, local copies, waits for them, and re-layouts: none -> 11.5 us  [shards(): jnp.concatenate(lax.all_gather(down_weight, 'sp'), axis=1)]
    all_gather x1, waiting for transfers between devices: 15.5 us -> 4.74 us  [shards(): whole_rows = lax.all_gather(normed, 'tp', axis=0, tiled=True)]
  transfers between devices with their start and end apart: 5 -> 5, of which waited for: 5 -> 5; matrix products, arithmetic and copies ran while one was open for 0% -> 3% of each run, Pallas kernels for 0% -> 0%
where the time goes in v1:
time: 456 us; the launch traced here: 455 us
  waiting for transfers between devices  327 us (72%)
  blocking collectives  62.9 us (14%)
  local copies, waits for them, and re-layouts  24.7 us (5%)
  matrix products  18 us (4%)
  between operations  15.3 us (3%)
  other arithmetic  6.74 us (1%)
    all_gather x1, waiting for transfers between devices, shards(): up_collected = lax.all_gather(up_weight, 'sp', axis=0, tiled=True)  151 us
    all_gather x1, waiting for transfers between devices, shards(): lax.all_gather(down_weight, 'sp')  123 us
    reduce_scatter x1, waiting for transfers between devices, shards(): lax.psum_scatter((jnp.dot(att_narrow, out_narrow, preferred_element_type=...  24.4 us
    reduce_scatter x1, waiting for transfers between devices, shards(): lax.psum_scatter(partials.astype(jnp.bfloat16), 'tp', scatter_dimension=0...  23.1 us
    all_gather x1, blocking collectives, attend(): wide_keys = lax.all_gather(key_wide, 'sp', axis=0, tiled=True)  17.7 us
    all_gather x1, blocking collectives, attend(): narrow_values = lax.all_gather(value_narrow, 'sp', axis=0, tiled=True)  15.6 us
    all_gather x1, blocking collectives, attend(): wide_values = lax.all_gather(value_wide, 'sp', axis=0, tiled=True)  15.3 us
    all_gather x1, blocking collectives, attend(): narrow_keys = lax.all_gather(key_narrow, 'sp', axis=0, tiled=True)  14.2 us
  transfers between devices with their start and end apart: 5, of which 5 were waited for; matrix products, arithmetic and copies ran while one was open for 3% of the time, Pallas kernels for 0%

profile of v1, /device:TPU:0, one launch (start us, length us, event | category | flops | bytes accessed | tf_op | source)
XLA Modules:
  0.0 455.4 jit_solution(3938996647065552609)
XLA Ops:
  7.4 17.7 %all_gather.26 = bf16[1024,1,256]{2,0,1:T(8,128)(2,1)S(1)} all-gather(bf16[256,1,256]{2,0,1:T(8,128)(2,1)} %param.24), channel_id=1, replica_groups=mesh['grp'=2,'sp'=4,'tp'=4] {'sp'}, dimensions={0}, use_global_device_ids=true | all-gather | bytes 655360 | tf_op jit(solution)/shard_map/all_gather | solution.py:91
  25.1 0.1 reshape.262
  25.3 1.1 copy.48
  26.4 0.2 copy.50
  26.6 15.3 %all_gather.27 = bf16[1024,1,128]{2,0,1:T(8,128)(2,1)} all-gather(bf16[256,1,128]{2,0,1:T(8,128)(2,1)S(1)} %copy-done.13), channel_id=1, replica_groups=mesh['grp'=2,'sp'=4,'tp'=4] {'sp'}, dimensions={0}, use_global_device_ids=true | all-gather | bytes 327680 | tf_op jit(solution)/shard_map/all_gather | solution.py:92
  41.9 7.7 %while.31 = (s32[]{:T(128)}, f32[1,2,2,256]{3,1,2,0:T(2,128)S(1)}, f32[1,2,2,256]{3,1,2,0:T(2,128)S(1)}, f32[1,2,2,256,128]{4,3,2,1,0:T(8,128)}, bf16[2,512,1,2,...) while((s32[]{:T(128)}, f32[1,2,2,256]{3,1,2,0:T(2,128)S(1)}, ...), condition=%wide.region_8.9_spmd.clone, body=%wide.region_5.0_spmd.clone.sunk | while | flops 271980544 | bytes 18026748 | solution.py:53
  41.9 0.2 constant_dynamic-slice_fusion.2
  42.1 0.6 copy-done.1
  42.7 0.4 bitcast_reduce_fusion.5
  43.2 0.4 fusion.71
  43.7 0.6 copy-done.8
  44.2 0.1 copy-done.11
  44.3 0.6 fusion.72
  44.9 0.8 copy-done.9
  45.8 0.2 constant_dynamic-slice_fusion.2
  46.0 0.6 copy-done.1
  46.6 0.4 bitcast_reduce_fusion.5
  47.1 0.4 fusion.71
  47.5 0.6 copy-done.8
  48.1 0.1 copy-done.11
  48.1 0.6 fusion.72
  48.8 0.8 copy-done.9
  49.6 0.6 slice_bitcast_fusion.5
  50.2 14.2 %all_gather.24 = bf16[1024,1,128]{2,0,1:T(8,128)(2,1)S(1)} all-gather(bf16[256,1,128]{2,0,1:T(8,128)(2,1)S(1)} %copy-done.14), channel_id=1, replica_groups=mesh['grp'=2,'sp'=4,'tp'=4] {'sp'}, dimensions={0}, use_global_device_ids=true | all-gather | bytes 327680 | tf_op jit(solution)/shard_map/all_gather | solution.py:89
  64.4 0.2 reshape.281
  64.6 0.4 copy.44
  65.0 15.6 %all_gather.25 = bf16[1024,1,128]{2,0,1:T(8,128)(2,1)} all-gather(bf16[256,1,128]{2,0,1:T(8,128)(2,1)} %param.22), channel_id=1, replica_groups=mesh['grp'=2,'sp'=4,'tp'=4] {'sp'}, dimensions={0}, use_global_device_ids=true | all-gather | bytes 327680 | tf_op jit(solution)/shard_map/all_gather | solution.py:90
  80.7 0.1 copy.43
  80.8 6.2 %while.30 = (s32[]{:T(128)}, f32[1,2,2,256]{3,1,2,0:T(2,128)S(1)}, f32[1,2,2,256]{3,1,2,0:T(2,128)S(1)}, f32[1,2,2,256,128]{4,3,2,1,0:T(8,128)}, bf16[2,512,1,2,...) while((s32[]{:T(128)}, f32[1,2,2,256]{3,1,2,0:T(2,128)S(1)}, ...), condition=%wide.region_3.4_spmd.clone, body=%wide.region_0.3_spmd.clone.sunk | while | flops 204871680 | bytes 13045957 | solution.py:53
  80.8 0.5 bitcast_reduce_fusion.4
  81.4 0.4 fusion.66
  81.8 0.6 copy-done.6
  82.4 0.1 copy-done.10
  82.5 0.6 fusion.67
  83.1 0.8 copy-done.7
  83.9 0.5 bitcast_reduce_fusion.4
  84.5 0.4 fusion.66
  84.9 0.6 copy-done.6
  85.5 0.1 copy-done.10
  85.5 0.6 fusion.67
  86.2 0.8 copy-done.7
  87.0 1.2 copy.51
  88.3 1.2 copy.46
  89.6 0.2 multiply_reduce_fusion
  89.8 0.1 multiply_convert_fusion
  89.9 0.5 fusion.45
  90.4 0.6 copy-done.5
  91.0 1.5 fusion.29
  92.5 0.0 all-gather.9.cloned.1.call-start
  92.5 0.5 all-gather.9.cloned.1.call-update
  93.0 0.0 all-gather.5.cloned.1.call-start
  93.1 24.4 %reduce-scatter.3.cloned.1.call-done = bf16[64,2048]{1,0:T(8,128)(2,1)} async-done(((bf16[256,2048]{1,0:T(8,128)(2,1)}), bf16[64,2048]{1,0:T(8,128)(2,1)}) %reduce-scatter.3.cloned.1.call-update) | async-done | bytes 262160 | tf_op jit(solution)/shard_map/reduce_scatter | solution.py:129
  117.5 1.1 fusion.30
  118.7 1.8 fusion.32
  120.5 0.0 all-gather.7.cloned.1.call-start
  120.5 0.5 all-gather.7.cloned.1.call-update
  121.0 0.0 reduce-scatter.5.cloned.1.call-start
  121.1 123.0 %all-gather.9.cloned.1.call-done = bf16[8192,512]{1,0:T(8,128)(2,1)} async-done(((bf16[2048,512]{1,0:T(8,128)(2,1)}), bf16[8192,512]{1,0:T(8,128)(2,1)}) %all-gather.9.cloned.1.call-update) | async-done | bytes 8388624 | tf_op jit(solution)/shard_map/all_gather | solution.py:150
  244.1 11.5 %copy.53 = bf16[2048,4,512]{0,2,1:T(8,128)(2,1)} copy(bf16[2048,4,512]{2,0,1:T(8,128)(2,1)} %bitcast.201) | data formatting | bytes 16777216 | tf_op jit(solution)/shard_map/reshape | solution.py:150
  255.6 4.7 %all-gather.5.cloned.1.call-done = bf16[256,2048]{1,0:T(8,128)(2,1)} async-done(((bf16[64,2048]{1,0:T(8,128)(2,1)}), bf16[256,2048]{1,0:T(8,128)(2,1)}) %all-gather.5.cloned.1.call-update) | async-done | bytes 1048592 | tf_op jit(solution)/shard_map/all_gather | solution.py:144
  260.3 150.9 %all-gather.7.cloned.1.call-done = bf16[2048,2048]{1,0:T(8,128)(2,1)} async-done(((bf16[512,2048]{1,0:T(8,128)(2,1)}), bf16[2048,2048]{1,0:T(8,128)(2,1)}) %all-gather.7.cloned.1.call-update) | async-done | bytes 8388624 | tf_op jit(solution)/shard_map/all_gather | solution.py:145
  411.3 11.7 %convolution_convert_fusion = bf16[256,2048]{1,0:T(8,128)(2,1)} fusion(bf16[2048,2048]{0,1:T(8,128)(2,1)} %bitcast.202, bf16[256,2048]{1,0:T(8,128)(2,1)} %all-gather.5.cloned.1.call-done, bf16[2048,2048]{1,0:T(8,128)(2,1)} %all-gather.7.cloned.1.call-done), kind=kOutput, calls=%fused_computation.52 | convolution fusion | flops 4297064448 | bytes 18874368 | tf_op jit(solution)/shard_map/dot_general | solution.py:148
  423.0 23.1 %reduce-scatter.5.cloned.1.call-done = bf16[64,2048]{1,0:T(8,128)(2,1)} async-done(((bf16[256,2048]{1,0:T(8,128)(2,1)}), bf16[64,2048]{1,0:T(8,128)(2,1)}) %reduce-scatter.5.cloned.1.call-update) | async-done | bytes 262160 | tf_op jit(solution)/shard_map/reduce_scatter | solution.py:153
  446.1 1.7 fusion.33
  (73 shorter events, 0.4 us)
Async XLA Ops:
  7.4 82.6 %copy-start = (bf16[256,2048]{1,0:T(8,128)(2,1)S(1)}, bf16[256,2048]{1,0:T(8,128)(2,1)}, u32[]{:S(2)}) copy-start(bf16[256,2048]{1,0:T(8,128)(2,1)} %param.29) | copy-start | bytes 3145732
  7.4 19.2 %copy-start.13 = (bf16[256,1,128]{2,0,1:T(8,128)(2,1)S(1)}, bf16[256,1,128]{2,0,1:T(8,128)(2,1)}, u32[]{:S(2)}) copy-start(bf16[256,1,128]{2,0,1:T(8,128)(2,1)} %param.25) | copy-start | bytes 196612
  7.4 110.1 %reduce-scatter.3.cloned.1.call-start = ((), (), s32[]{:S(2)}) async-start(), calls=%async_computation.2 | async-start | bytes 1310720 | tf_op jit(solution)/shard_map/reduce_scatter | solution.py:129
  41.9 8.3 %copy-start.14 = (bf16[256,1,128]{2,0,1:T(8,128)(2,1)S(1)}, bf16[256,1,128]{2,0,1:T(8,128)(2,1)}, u32[]{:S(2)}) copy-start(bf16[256,1,128]{2,0,1:T(8,128)(2,1)} %param.21) | copy-start | bytes 196612
  41.9 0.8 copy-start.1
  43.2 1.0 copy-start.8
  43.2 1.1 copy-start.11
  43.6 2.1 copy-start.2
  44.9 0.8 copy-start.9
  45.8 0.8 copy-start.1
  47.0 1.0 copy-start.8
  47.0 1.1 copy-start.11
  47.5 2.1 copy-start.2
  48.8 0.8 copy-start.9
  49.6 31.1 %copy-start.12 = (bf16[256,2,128]{2,1,0:T(2,128)(2,1)S(1)}, bf16[256,2,128]{2,1,0:T(2,128)(2,1)}, u32[]{:S(2)}) copy-start(bf16[256,2,128]{2,1,0:T(2,128)(2,1)} %param.20) | copy-start | bytes 393220
  81.3 1.0 copy-start.6
  81.4 1.1 copy-start.10
  83.1 0.8 copy-start.7
  84.4 1.0 copy-start.6
  84.4 1.1 copy-start.10
  86.2 0.8 copy-start.7
  87.0 2.6 copy-start.15
  87.0 2.6 copy-start.17
  87.0 2.6 copy-start.18
  87.0 2.8 copy-start.19
  89.8 1.2 copy-start.5
  92.4 0.7 copy-start.16
  92.4 25.1 %copy-start.3 = (bf16[64,2048]{1,0:T(8,128)(2,1)S(1)}, bf16[64,2048]{1,0:T(8,128)(2,1)}, u32[]{:S(2)}) copy-start(bf16[64,2048]{1,0:T(8,128)(2,1)} %param.19) | copy-start | bytes 786436
  92.5 151.6 %all-gather.9.cloned.1.call-start = ((), (), s32[]{:S(2)}) async-start(), calls=%async_computation.6 | async-start | bytes 10485760 | tf_op jit(solution)/shard_map/all_gather | solution.py:150
  93.0 167.3 %all-gather.5.cloned.1.call-start = ((), (), s32[]{:S(2)}) async-start(), calls=%async_computation.3 | async-start | bytes 1310720 | tf_op jit(solution)/shard_map/all_gather | solution.py:144
  120.5 290.8 %all-gather.7.cloned.1.call-start = ((), (), s32[]{:S(2)}) async-start(), calls=%async_computation.4 | async-start | bytes 10485760 | tf_op jit(solution)/shard_map/all_gather | solution.py:145
  121.0 325.1 %reduce-scatter.5.cloned.1.call-start = ((), (), s32[]{:S(2)}) async-start(), calls=%async_computation.5 | async-start | bytes 1310720 | tf_op jit(solution)/shard_map/reduce_scatter | solution.py:153
  411.3 34.8 %copy-start.4 = (bf16[64,2048]{1,0:T(8,128)(2,1)S(1)}, bf16[64,2048]{1,0:T(8,128)(2,1)}, u32[]{:S(2)}) copy-start(bf16[64,2048]{1,0:T(8,128)(2,1)} %reduce-scatter.3.cloned.1.call-done) | copy-start | bytes 786436
Sparse Core Ops, SparseCore 0:
  92.6 24.8 reduce-scatter.2
  423.1 22.9 reduce-scatter.4
Sparse Core Ops, SparseCore 1:
  94.5 149.5 all-gather.8
  245.5 14.7 all-gather.4
  261.8 149.4 all-gather.6
